TPU v7x, 32 devices: a whole 2x2x4 slice. The times are simulated.
32 devices in a mesh: dp: 4 (over y, x), kv: 4 (over z), tp: 2 (over core).
Axes of the slice: x: 2, y: 2, z: 4, core: 2. Of those that a mesh axis runs over, the one named last changes fastest.
Arguments:
- piece_tokens: bfloat16 [2048, 2048], P(('dp', 'kv')), parts along dimension 0, may hold values from -6 to 6
- step_tokens: bfloat16 [16, 2048], P(('dp', 'kv')), parts along dimension 0, may hold values from -6 to 6
- norm_gain: float32 [2048], replicated, may hold values from 0.1 to 1.9
- query_weight: bfloat16 [2048, 1024], P(None, 'tp'), may hold values from -0.125 to 0.125
- key_weight: bfloat16 [2048, 1024], P(None, 'tp'), may hold values from -0.125 to 0.125
- value_weight: bfloat16 [2048, 1024], P(None, 'tp'), may hold values from -0.125 to 0.125
- gate_weight: bfloat16 [2048, 16], replicated, may hold values from -0.125 to 0.125
- gate_bias: float32 [16], replicated, may hold values from 3 to 10.5
- out_weight: bfloat16 [1024, 2048], P(None, 'tp'), may hold values from -0.1875 to 0.1875
- cache_keys: bfloat16 [8192, 1024], P(('dp', 'kv'), 'tp'), parts along dimension 0, may hold values from -320 to 320
- cache_values: bfloat16 [8192, 1024], P(('dp', 'kv'), 'tp'), parts along dimension 0, may hold values from -10 to 10
- cache_decay: float32 [16, 8192], P('tp', ('dp', 'kv')), parts along dimension 1, may hold values from -696.32 to 0, as said below
- decay_total: float32 [64], P('dp'), parts along dimension 0, may hold values from -696.32 to 0, as said below
- step_keys: bfloat16 [16, 1024, 1024], P(('dp', 'kv'), None, 'tp'), parts along dimension 0, may hold values from -6 to 6
- step_values: bfloat16 [16, 1024, 1024], P(('dp', 'kv'), None, 'tp'), parts along dimension 0, may hold values from -6 to 6
- step_gates: float32 [16, 16, 1024], P(('dp', 'kv'), 'tp'), parts along dimension 0, may hold values from -0.34 to 0
- step_lengths: int32 [16], P(('dp', 'kv')), parts along dimension 0, may hold values from 1 to 1024, 2048 in all
Outputs:
- piece_out: bfloat16 [2048, 2048], P(('dp', 'kv'), 'tp'), parts along dimension 0
- step_out: bfloat16 [16, 2048], P(('dp', 'kv'), 'tp'), parts along dimension 0
There are 4 independent parts, one for each index of `dp`. A program takes and returns all parts, laid end to end along the dimension named above; an argument that names none is the same for every part. Nothing has to cross between parts.
Inputs may be any that keep to these rules, and one draw needn't show every extreme that they name: `cache_decay`: cumulative values never rise along the positions and start at one gate below zero. `decay_total`: equal to the cumulative value of the last cached position. `step_lengths`: each length is 1 to 1024; the largest is exactly 1024; positions at or past a length are unused.
All inputs are finite; a program needn't handle non-finite values.
Results may differ from a plain program's by a relative error of at most 0.0095.
The roundings to bfloat16 on the way count: a program that leaves them out, or rounds other values in their place, can miss the bound.
Values may be sent and summed in bfloat16 or wider, within the bound.
A program may use at most 128 MiB of HBM per device.

v0:
```python
import jax
import jax.numpy as jnp
from jax import lax
from jax.sharding import PartitionSpec as P

norm_eps = 1e-06
negative = -1e30


def carried_in(value, axis, join, neutral):
    count, mine = (lax.axis_size(axis), lax.axis_index(axis))
    pieces = lax.all_gather(value, axis)
    total = jnp.full_like(value, 0) + jnp.asarray(neutral, value.dtype)

    def step(position, total):
        longer = join(total, pieces[position])
        return jnp.where(position < mine, longer, total)

    return lax.fori_loop(0, count - 1, step, total)


def normalize(token_rows, norm_gain):
    wide = token_rows.astype(jnp.float32)
    factor = lax.rsqrt(jnp.mean(wide * wide, axis=-1, keepdims=True) + norm_eps)
    return (wide * factor * norm_gain).astype(jnp.bfloat16)


def attend_piece(queries, positions, all_keys, all_values, key_bias, key_slots, cache_len):
    head_count = key_bias.shape[0]
    query_count = queries.shape[0]
    head_width = all_keys.shape[1] // head_count
    score_scale = head_width ** (-0.5)
    key_heads = all_keys.reshape(all_keys.shape[0], head_count, head_width)
    value_heads = all_values.reshape(all_values.shape[0], head_count, head_width)

    def one_block(block_args):
        block_q, block_pos = block_args
        row_count = block_q.shape[0]
        scores = (
            jnp.einsum(
                "qhd,khd->hqk",
                block_q.reshape(row_count, head_count, head_width),
                key_heads,
                preferred_element_type=jnp.float32,
            )
            * score_scale
        )
        scores = scores + key_bias[:, None, :]
        visible = jnp.concatenate(
            [jnp.ones((row_count, cache_len), jnp.bool_), block_pos[:, None] >= key_slots[None, :]],
            axis=1,
        )
        scores = jnp.where(visible[None], scores, negative)
        row_high = jnp.max(scores, axis=-1)
        exp_scores = jnp.exp(scores - row_high[..., None])
        row_mass = jnp.sum(exp_scores, axis=-1)
        summed = jnp.einsum(
            "hqk,khd->qhd",
            exp_scores.astype(jnp.bfloat16),
            value_heads,
            preferred_element_type=jnp.float32,
        )
        part_means = (
            (summed / row_mass.T[:, :, None])
            .astype(jnp.bfloat16)
            .reshape(row_count, head_count * head_width)
        )
        return (part_means, row_high.T, row_mass.T)

    if query_count > 512 and query_count % 512 == 0:
        group_count = query_count // 512
        part_means, part_high, part_mass = lax.map(
            one_block, (queries.reshape(group_count, 512, -1), positions.reshape(group_count, 512))
        )
        return (
            part_means.reshape(query_count, -1),
            part_high.reshape(query_count, head_count),
            part_mass.reshape(query_count, head_count),
        )
    return one_block((queries, positions))


def combine(part_means, part_high, part_mass):
    best_high = jnp.max(part_high, axis=0)
    share = part_mass * jnp.exp(part_high - best_high[None])
    peer_count, row_count, head_count = share.shape
    part_float = part_means.reshape(peer_count, row_count, head_count, -1).astype(jnp.float32)
    summed = jnp.sum(share[..., None] * part_float, axis=0) / jnp.sum(share, axis=0)[..., None]
    return summed.astype(jnp.bfloat16).reshape(row_count, -1)


def per_device(
    piece_tokens,
    step_tokens,
    norm_gain,
    query_weight,
    key_weight,
    value_weight,
    gate_weight,
    gate_bias,
    out_weight,
    cache_keys,
    cache_values,
    cache_decay,
    decay_total,
    step_keys,
    step_values,
    step_gates,
    step_lengths,
):
    piece_rows = piece_tokens.shape[0]
    step_count = step_tokens.shape[0]
    head_count = cache_decay.shape[0]
    head_width = query_weight.shape[1] // head_count
    score_scale = head_width ** (-0.5)
    head_start = lax.axis_index("tp") * head_count
    token_rows = jnp.concatenate([piece_tokens, step_tokens], axis=0)
    normed = normalize(token_rows, norm_gain)
    queries = jnp.dot(normed, query_weight, preferred_element_type=jnp.float32).astype(jnp.bfloat16)
    new_keys = jnp.dot(normed, key_weight, preferred_element_type=jnp.float32).astype(jnp.bfloat16)
    new_values = jnp.dot(normed, value_weight, preferred_element_type=jnp.float32).astype(
        jnp.bfloat16
    )
    gate_cols = lax.dynamic_slice_in_dim(gate_weight, head_start, head_count, 1)
    bias_cols = lax.dynamic_slice_in_dim(gate_bias, head_start, head_count, 0)
    start_decay = lax.dynamic_slice_in_dim(decay_total, head_start, head_count, 0)
    log_gates = jax.nn.log_sigmoid(
        jnp.dot(normed, gate_cols, preferred_element_type=jnp.float32) + bias_cols
    )
    piece_gates = log_gates[:piece_rows]
    gate_before = carried_in(
        jnp.sum(piece_gates, axis=0), "kv", jnp.add, jnp.zeros((head_count,), jnp.float32)
    )
    piece_decay = start_decay + gate_before + jnp.cumsum(piece_gates, axis=0)
    key_bias = -jnp.concatenate([cache_decay, piece_decay.T], axis=1)
    all_keys = jnp.concatenate([cache_keys, new_keys[:piece_rows]], axis=0)
    all_values = jnp.concatenate([cache_values, new_values[:piece_rows]], axis=0)
    key_slots = lax.axis_index("kv") * piece_rows + jnp.arange(piece_rows, dtype=jnp.int32)
    cache_len = cache_keys.shape[0]
    peer_count = lax.axis_size("kv")
    own_queries = queries[:piece_rows]
    gathered = lax.all_gather(own_queries, "kv", axis=0, tiled=True)
    positions = jnp.arange(peer_count * piece_rows, dtype=jnp.int32)
    part_means, part_high, part_mass = attend_piece(
        gathered, positions, all_keys, all_values, key_bias, key_slots, cache_len
    )
    part_means = lax.all_to_all(part_means[None], "kv", split_axis=1, concat_axis=0, tiled=True)
    part_high, part_mass = (
        lax.all_to_all(part_high[None], "kv", split_axis=1, concat_axis=0, tiled=True),
        lax.all_to_all(part_mass[None], "kv", split_axis=1, concat_axis=0, tiled=True),
    )
    piece_att = combine(part_means, part_high, part_mass)
    cache_span = step_keys.shape[1]
    step_q = queries[piece_rows:].reshape(step_count, head_count, head_width)
    step_k = new_keys[piece_rows:].reshape(step_count, head_count, head_width)
    step_v = new_values[piece_rows:].reshape(step_count, head_count, head_width)
    step_lg = log_gates[piece_rows:]
    in_cache = jnp.arange(cache_span, dtype=jnp.int32)[None, :] < step_lengths[:, None]
    kept_gates = jnp.where(in_cache[:, None, :], step_gates, 0.0)
    running = jnp.cumsum(kept_gates, axis=2)
    after_sum = running[:, :, -1:] - running
    cache_scores = (
        jnp.einsum(
            "bhd,blhd->bhl",
            step_q,
            step_keys.reshape(step_count, cache_span, head_count, head_width),
            preferred_element_type=jnp.float32,
        )
        * score_scale
    )
    cache_scores = cache_scores + step_lg[:, :, None] + after_sum
    cache_scores = jnp.where(in_cache[:, None, :], cache_scores, negative)
    self_scores = (
        jnp.einsum("bhd,bhd->bh", step_q, step_k, preferred_element_type=jnp.float32) * score_scale
    )
    step_high = jnp.maximum(jnp.max(cache_scores, axis=-1), self_scores)
    cache_exp = jnp.exp(cache_scores - step_high[..., None])
    self_exp = jnp.exp(self_scores - step_high)
    step_mass = jnp.sum(cache_exp, axis=-1) + self_exp
    step_mix = jnp.einsum(
        "bhl,blhd->bhd",
        cache_exp.astype(jnp.bfloat16),
        step_values.reshape(step_count, cache_span, head_count, head_width),
        preferred_element_type=jnp.float32,
    )
    step_mix = step_mix + self_exp.astype(jnp.bfloat16).astype(jnp.float32)[
        ..., None
    ] * step_v.astype(jnp.float32)
    step_att = (
        (step_mix / step_mass[..., None])
        .astype(jnp.bfloat16)
        .reshape(step_count, head_count * head_width)
    )
    att_rows = jnp.concatenate([piece_att, step_att], axis=0)
    projected = jnp.dot(
        lax.all_gather(att_rows, "tp", axis=1, tiled=True),
        out_weight,
        preferred_element_type=jnp.float32,
    )
    projected = projected.astype(jnp.bfloat16)
    return (projected[:piece_rows], projected[piece_rows:])


def solution(mesh):
    in_specs = (
        P(("dp", "kv"), None),
        P(("dp", "kv"), None),
        P(),
        P(None, "tp"),
        P(None, "tp"),
        P(None, "tp"),
        P(),
        P(),
        P(None, "tp"),
        P(("dp", "kv"), "tp"),
        P(("dp", "kv"), "tp"),
        P("tp", ("dp", "kv")),
        P("dp"),
        P(("dp", "kv"), None, "tp"),
        P(("dp", "kv"), None, "tp"),
        P(("dp", "kv"), "tp", None),
        P(("dp", "kv")),
    )
    out_specs = (P(("dp", "kv"), "tp"), P(("dp", "kv"), "tp"))
    return jax.shard_map(
        per_device, mesh=mesh, in_specs=in_specs, out_specs=out_specs, check_vma=False
    )
```

profile of v0, /device:TPU:0, one launch (start us, length us, event | category | flops | bytes accessed | tf_op | source)
XLA Modules:
  0.0 125.6 jit_solution(8513010429715983522)
XLA Ops:
  2.9 1.5 %fusion.25 = f32[129,8]{0,1:T(8,128)S(1)} fusion(bf16[2048,16]{0,1:T(8,128)(2,1)} %param.25, s32[]{:T(128)S(6)} %select_n.43, f32[8]{0:T(128)S(1)} %dynamic_slice.18, f32[2048]{0:T(1024)} %param.21, f32[129]{0:T(256)S(1)} %add_rsqrt_fusion, bf16[1,2048]{1,0:T(2,128)(2,1)} %param.20, bf16[128,2048]{1,0:T(8,128)(2,1)} %param.19), kind=kOutput, calls=%fused_computation.49 | convolution fusion | flops 6085704 | bytes 578120 | tf_op jit(solution)/shard_map/dot_general | solution.py:128
  6.1 13.5 %all-reduce.1 = f32[32]{0:T(128)S(1)} all-reduce(f32[32]{0:T(128)S(1)} %dynamic-update-slice), channel_id=2, replica_groups=mesh['dp'=4,'kv'=4,'tp'=2] {'kv'}, use_global_device_ids=true, to_apply=%add.1 | all-reduce | flops 32 | bytes 256
  20.3 2.1 %convolution_convert_fusion.2 = bf16[129,512]{1,0:T(8,128)(2,1)S(1)} fusion(bf16[2048,512]{1,0:T(8,128)(2,1)} %param.23, f32[2048]{0:T(1024)S(1)} %copy-done.20, f32[129]{0:T(256)S(1)} %add_rsqrt_fusion, bf16[1,2048]{1,0:T(2,128)(2,1)S(1)} %copy-done.13, bf16[128,2048]{1,0:T(8,128)(2,1)S(1)} %copy-done.3), kind=kOutput, calls=%fused_computation.14 | convolution fusion | flops 272448000 | bytes 2766340 | tf_op jit(solution)/shard_map/dot_general | solution.py:120
  23.5 2.3 %convolution_convert_fusion.3 = bf16[129,512]{1,0:T(8,128)(2,1)S(1)} fusion(bf16[2048,512]{1,0:T(8,128)(2,1)} %param.22, f32[2048]{0:T(1024)S(1)} %copy-done.20, f32[129]{0:T(256)S(1)} %add_rsqrt_fusion, bf16[1,2048]{1,0:T(2,128)(2,1)S(1)} %copy-done.13, bf16[128,2048]{1,0:T(8,128)(2,1)} %param.19), kind=kOutput, calls=%fused_computation.15 | convolution fusion | flops 272448000 | bytes 2766340 | tf_op jit(solution)/shard_map/dot_general | solution.py:119
  26.5 14.8 %all_gather.12 = bf16[512,512]{1,0:T(8,128)(2,1)S(1)} all-gather(bf16[128,512]{1,0:T(8,128)(2,1)S(1)} %slice.52), channel_id=1, replica_groups=mesh['dp'=4,'kv'=4,'tp'=2] {'kv'}, dimensions={0}, use_global_device_ids=true | all-gather | bytes 655360 | tf_op jit(solution)/shard_map/all_gather | solution.py:142
  41.6 3.8 %fusion.2 = (f32[8,512]{1,0:T(8,128)S(1)}, f32[8,512,640]{2,1,0:T(8,128)S(1)}) fusion(f32[8,640]{1,0:T(8,128)S(1)} %maximum_negate_fusion, pred[512,640]{1,0:T(8,128)(4,1)S(1)} %concatenate.22, bf16[512,8,64]{0,2,1:T(8,128)(2,1)S(1)} %bitcast.94, bf16[640,8,64]{0,2,1:T(8,128)(2,1)} %bitcast.91), kind=kOutput, calls=%fused_computation.6 | convolution fusion | flops 346025984 | bytes 12029952 | tf_op jit(solution)/shard_map/qhd,khd->hqk/dot_general | solution.py:40
  45.4 2.9 %fusion.1 = f32[8,512]{1,0:T(8,128)S(1)} fusion(f32[8,512,640]{2,1,0:T(8,128)S(1)} %get-tuple-element.116, f32[8,512]{1,0:T(8,128)S(1)} %get-tuple-element.115, f32[8,640]{1,0:T(8,128)S(1)} %maximum_negate_fusion, pred[512,640]{1,0:T(8,128)(4,1)S(1)} %concatenate.22), kind=kLoop, calls=%fused_computation.5 | loop fusion | flops 13103104 | bytes 10866688 | tf_op jit(solution)/shard_map/reduce_sum | solution.py:56
  52.1 4.0 %all-to-all-start = ((f32[4,1,1024]{2,1,0:T(1,128)}), f32[4,1,1024]{2,1,0:T(1,128)}, u32[]{:S(2)}, u32[]{:S(2)}) async-start(f32[4,1,1024]{2,1,0:T(1,128)} %reshape.272), calls=%async_computation | async-start | bytes 32768 | tf_op jit(solution)/shard_map/all_to_all | solution.py:150
  57.6 2.3 %reduce-window.6 = f32[1,8,8,128]{3,2,1,0:T(8,128)S(1)} reduce-window(f32[1,8,8,128]{3,2,1,0:T(8,128)S(1)} %copy.135, f32[]{:T(128)} %constant.56.clone.1), window={size=1x1x1x128 pad=0_0x0_0x0_0x127_0}, to_apply=%region_10.11 | reduce-window | flops 1040384 | bytes 65540 | tf_op jit(solution)/shard_map/reduce-window
  63.2 2.1 %convolution_convert_fusion.1 = bf16[129,512]{1,0:T(8,128)(2,1)S(1)} fusion(bf16[2048,512]{1,0:T(8,128)(2,1)} %param.24, f32[2048]{0:T(1024)} %param.21, f32[129]{0:T(256)} %copy-done.18, bf16[1,2048]{1,0:T(2,128)(2,1)} %param.20, bf16[128,2048]{1,0:T(8,128)(2,1)S(1)} %copy-done.4), kind=kOutput, calls=%fused_computation.13 | convolution fusion | flops 272448000 | bytes 2766340 | tf_op jit(solution)/shard_map/dot_general | solution.py:121
  68.5 1.5 %copy.134 = bf16[1,1024,512]{1,2,0:T(8,128)(2,1)S(1)} copy(bf16[1,1024,512]{2,1,0:T(8,128)(2,1)} %param.32) | data formatting | bytes 2097152 | tf_op args[13]
  71.3 6.7 %divide_convert_fusion = bf16[512,8,64]{0,2,1:T(8,128)(2,1)} fusion(bf16[640,8,64]{0,2,1:T(8,128)(2,1)} %bitcast.90, f32[8,512,640]{2,1,0:T(8,128)} %copy-done.1, f32[8,512]{1,0:T(8,128)S(1)} %get-tuple-element.115, f32[8,640]{1,0:T(8,128)S(1)} %copy-done.9, pred[512,640]{1,0:T(8,128)(4,1)S(1)} %concatenate.22, f32[512,8]{0,1:T(8,128)} %bitcast.99), kind=kOutput, calls=%fused_computation.22 | convolution fusion | flops 349175808 | bytes 12046336 | tf_op jit(solution)/shard_map/hqk,khd->qhd/dot_general | solution.py:57
  81.7 4.9 %all-to-all-start.1 = ((f32[4,1,1024]{2,1,0:T(1,128)}), f32[4,1,1024]{2,1,0:T(1,128)S(1)}, u32[]{:S(2)}, u32[]{:S(2)}) async-start(f32[4,1,1024]{2,1,0:T(1,128)} %reshape.274), calls=%async_computation.1 | async-start | bytes 32768 | tf_op jit(solution)/shard_map/all_to_all | solution.py:149
  86.5 2.4 %copy.130 = bf16[1,512,512]{2,0,1:T(2,128)(2,1)S(1)} copy(bf16[1,512,512]{1,2,0:T(8,128)(2,1)} %bitcast.92) | data formatting | bytes 1048576 | tf_op jit(solution)/shard_map/broadcast_in_dim;reshape | solution.py:147
  89.5 4.6 %reduce.21 = bf16[512,512]{1,0:T(8,128)(2,1)} reduce(bf16[512,1,512]{2,1,0:T(2,128)(2,1)S(1)} %bitcast.82, bf16[]{:T(256)} %broadcast.114), dimensions={1}, to_apply=%bitcast.58.reduce_sub_computation | reduce | bytes 1048578
  94.1 2.2 %reshape.270 = bf16[4,2,32768]{2,1,0:T(2,128)(2,1)} reshape(bf16[512,512]{1,0:T(8,128)(2,1)} %reduce.21) | data formatting | bytes 1048576
  96.3 1.5 %copy.139 = bf16[1,1024,512]{1,2,0:T(8,128)(2,1)S(1)} copy(bf16[1,1024,512]{2,1,0:T(8,128)(2,1)} %param.33) | data formatting | bytes 2097152 | tf_op args[14]
  97.8 5.1 %all-to-all-start.2 = ((bf16[4,2,32768]{2,1,0:T(2,128)(2,1)}), bf16[4,2,32768]{2,1,0:T(2,128)(2,1)}, u32[]{:S(2)}, u32[]{:S(2)}) async-start(bf16[4,2,32768]{2,1,0:T(2,128)(2,1)} %reshape.270), calls=%async_computation.2 | async-start | bytes 1048576 | tf_op jit(solution)/shard_map/all_to_all | solution.py:147
  104.5 1.4 %reduce.23 = f32[4,1024]{1,0:T(4,128)S(1)} reduce(f32[4,1,1024]{2,1,0:T(1,128)} %all-to-all-done, f32[]{:T(128)} %broadcast.115), dimensions={1}, to_apply=%all_to_all.10.reduce_sub_computation | reduce | bytes 32772 | tf_op jit(solution)/shard_map/all_to_all | solution.py:150
  107.8 5.5 %all-to-all-done.2 = bf16[4,2,32768]{2,1,0:T(2,128)(2,1)} async-done(((bf16[4,2,32768]{2,1,0:T(2,128)(2,1)}), bf16[4,2,32768]{2,1,0:T(2,128)(2,1)}, u32[]{:S(2)}, u32[]{:S(2)}) %all-to-all-start.2) | async-done | bytes 524320 | tf_op jit(solution)/shard_map/all_to_all | solution.py:147
  113.3 2.2 %reshape.271 = bf16[512,1,512]{2,1,0:T(2,128)(2,1)S(1)} reshape(bf16[4,2,32768]{2,1,0:T(2,128)(2,1)} %all-to-all-done.2) | data formatting | bytes 1048576
  116.6 2.6 %copy.132 = f32[1,512,512]{1,2,0:T(8,128)} copy(f32[1,512,512]{2,1,0:T(8,128)} %copy_convert_fusion) | data formatting | bytes 2097152 | tf_op jit(solution)/shard_map/convert_element_type | solution.py:87
  119.2 1.6 %reshape.241 = f32[4,128,8,64]{1,0,3,2:T(4,128)S(1)} reshape(f32[1,512,512]{1,2,0:T(8,128)} %copy.132) | data formatting | bytes 2097152 | tf_op jit(solution)/shard_map/convert_element_type | solution.py:87
  121.6 2.2 %all_gather.15 = bf16[129,1024]{0,1:T(8,128)(2,1)S(1)} all-gather(bf16[129,512]{0,1:T(8,128)(2,1)S(1)} %pad_maximum_fusion.3), channel_id=1, replica_groups=mesh['dp'=4,'kv'=4,'tp'=2] {'tp'}, dimensions={1}, use_global_device_ids=true | all-gather | bytes 396288 | tf_op jit(solution)/shard_map/all_gather | solution.py:196
  (125 shorter events, 29.6 us)
Async XLA Ops:
  0.6 123.1 %copy-start = (bf16[1024,1024]{1,0:T(8,128)(2,1)S(1)}, bf16[1024,1024]{1,0:T(8,128)(2,1)}, u32[]{:S(2)}) copy-start(bf16[1024,1024]{1,0:T(8,128)(2,1)} %param.27) | copy-start | bytes 6291460
  0.6 3.8 %copy-start.21 = (u32[32]{0:T(128)S(1)}, u32[32]{0:T(128)}, u32[]{:S(2)}) copy-start(u32[32]{0:T(128)} %constant.74) | copy-start | bytes 388
  0.7 19.6 %copy-start.3 = (bf16[128,2048]{1,0:T(8,128)(2,1)S(1)}, bf16[128,2048]{1,0:T(8,128)(2,1)}, u32[]{:S(2)}) copy-start(bf16[128,2048]{1,0:T(8,128)(2,1)} %param.19) | copy-start | bytes 1572868
  0.7 19.6 %copy-start.13 = (bf16[1,2048]{1,0:T(2,128)(2,1)S(1)}, bf16[1,2048]{1,0:T(2,128)(2,1)}, u32[]{:S(2)}) copy-start(bf16[1,2048]{1,0:T(2,128)(2,1)} %param.20) | copy-start | bytes 12292
  0.7 19.6 %copy-start.20 = (f32[2048]{0:T(1024)S(1)}, f32[2048]{0:T(1024)}, u32[]{:S(2)}) copy-start(f32[2048]{0:T(1024)} %param.21) | copy-start | bytes 24580
  0.7 19.3 %copy-start.19 = (f32[16]{0:T(128)S(1)}, f32[16]{0:T(128)}, u32[]{:S(2)}) copy-start(f32[16]{0:T(128)} %param.31) | copy-start | bytes 196
  2.1 21.4 %copy-start.18 = (f32[129]{0:T(256)}, f32[129]{0:T(256)S(1)}, u32[]{:S(2)}) copy-start(f32[129]{0:T(256)S(1)} %add_rsqrt_fusion) | copy-start | bytes 1552
  19.7 2.7 %copy-start.2 = (bf16[512,512]{1,0:T(8,128)(2,1)S(1)}, bf16[512,512]{1,0:T(8,128)(2,1)}, u32[]{:S(2)}) copy-start(bf16[512,512]{1,0:T(8,128)(2,1)} %param.28) | copy-start | bytes 1572868
  22.3 3.5 %copy-start.6 = (bf16[129,512]{1,0:T(8,128)(2,1)}, bf16[129,512]{1,0:T(8,128)(2,1)S(1)}, u32[]{:S(2)}) copy-start(bf16[129,512]{1,0:T(8,128)(2,1)S(1)} %convolution_convert_fusion.2) | copy-start | bytes 396292
  23.5 17.9 %copy-start.12 = (f32[8,512]{1,0:T(8,128)S(1)}, f32[8,512]{1,0:T(8,128)}, u32[]{:S(2)}) copy-start(f32[8,512]{1,0:T(8,128)} %param.30) | copy-start | bytes 49156
  25.8 0.7 copy-start.7
  41.5 3.9 %copy-start.8 = (f32[8,640]{1,0:T(8,128)}, f32[8,640]{1,0:T(8,128)S(1)}, u32[]{:S(2)}) copy-start(f32[8,640]{1,0:T(8,128)S(1)} %maximum_negate_fusion) | copy-start | bytes 61444
  45.3 4.0 %copy-start.1 = (f32[8,512,640]{2,1,0:T(8,128)}, f32[8,512,640]{2,1,0:T(8,128)S(1)}, u32[]{:S(2)}) copy-start(f32[8,512,640]{2,1,0:T(8,128)S(1)} %get-tuple-element.116) | copy-start | bytes 31457284
  45.4 12.2 %copy-start.11 = (f32[1,8,1024]{2,1,0:T(8,128)S(1)}, f32[1,8,1024]{2,1,0:T(8,128)}, u32[]{:S(2)}) copy-start(f32[1,8,1024]{2,1,0:T(8,128)} %param.34) | copy-start | bytes 98308
  45.4 17.8 %copy-start.4 = (bf16[128,2048]{1,0:T(8,128)(2,1)S(1)}, bf16[128,2048]{1,0:T(8,128)(2,1)}, u32[]{:S(2)}) copy-start(bf16[128,2048]{1,0:T(8,128)(2,1)} %param.19) | copy-start | bytes 1572868
  49.3 8.2 %copy-start.10 = (f32[8,512]{1,0:T(8,128)}, f32[8,512]{1,0:T(8,128)S(1)}, u32[]{:S(2)}) copy-start(f32[8,512]{1,0:T(8,128)S(1)} %fusion.1) | copy-start | bytes 49156
  52.1 29.5 %all-to-all-start = ((f32[4,1,1024]{2,1,0:T(1,128)}), f32[4,1,1024]{2,1,0:T(1,128)}, u32[]{:S(2)}, u32[]{:S(2)}) async-start(f32[4,1,1024]{2,1,0:T(1,128)} %reshape.272), calls=%async_computation | async-start | bytes 32768 | tf_op jit(solution)/shard_map/all_to_all | solution.py:150
  57.5 7.8 %copy-start.15 = (pred[1024]{0:T(1024)(128)(4,1)}, pred[1024]{0:T(1024)(128)(4,1)S(1)}, u32[]{:S(2)}) copy-start(pred[1024]{0:T(1024)(128)(4,1)S(1)} %iota_compare_fusion.1) | copy-start | bytes 3076
  66.0 5.2 %copy-start.9 = (f32[8,640]{1,0:T(8,128)S(1)}, f32[8,640]{1,0:T(8,128)}, u32[]{:S(2)}) copy-start(f32[8,640]{1,0:T(8,128)} %copy-done.8) | copy-start | bytes 61444
  71.2 7.6 %copy-start.14 = (bf16[8,64]{1,0:T(8,128)(2,1)S(1)}, bf16[8,64]{1,0:T(8,128)(2,1)}, u32[]{:S(2)}) copy-start(bf16[8,64]{1,0:T(8,128)(2,1)} %reshape.238) | copy-start | bytes 3076
  71.2 7.8 %copy-start.16 = (pred[1024]{0:T(1024)(128)(4,1)S(1)}, pred[1024]{0:T(1024)(128)(4,1)}, u32[]{:S(2)}) copy-start(pred[1024]{0:T(1024)(128)(4,1)} %copy-done.15) | copy-start | bytes 3076
  71.2 7.8 %copy-start.17 = (f32[8]{0:T(128)S(1)}, f32[8]{0:T(128)}, u32[]{:S(2)}) copy-start(f32[8]{0:T(128)} %slice_reduce_fusion.1) | copy-start | bytes 100
  81.7 16.1 %all-to-all-start.1 = ((f32[4,1,1024]{2,1,0:T(1,128)}), f32[4,1,1024]{2,1,0:T(1,128)S(1)}, u32[]{:S(2)}, u32[]{:S(2)}) async-start(f32[4,1,1024]{2,1,0:T(1,128)} %reshape.274), calls=%async_computation.1 | async-start | bytes 32768 | tf_op jit(solution)/shard_map/all_to_all | solution.py:149
  97.8 15.5 %all-to-all-start.2 = ((bf16[4,2,32768]{2,1,0:T(2,128)(2,1)}), bf16[4,2,32768]{2,1,0:T(2,128)(2,1)}, u32[]{:S(2)}, u32[]{:S(2)}) async-start(bf16[4,2,32768]{2,1,0:T(2,128)(2,1)} %reshape.270), calls=%async_computation.2 | async-start | bytes 1048576 | tf_op jit(solution)/shard_map/all_to_all | solution.py:147
  (1 other events, 0.7 us)
where the time goes:
time: 127 us; the launch traced here: 126 us
  local copies, waits for them, and re-layouts  31.8 us (25%)
  blocking collectives  30.4 us (24%)
  other arithmetic  21.8 us (17%)
  matrix products  19.5 us (15%)
  starting transfers between devices  14 us (11%)
  waiting for transfers between devices  5.55 us (4%)
  between operations  2.56 us (2%)
    all_gather x1, blocking collectives, per_device(): gathered = lax.all_gather(own_queries, 'kv', axis=0, tiled=True)  14.8 us
    unnamed x57, local copies, waits for them, and re-layouts  14.3 us
    unnamed x1, blocking collectives  13.5 us
    unnamed x4, other arithmetic  7.29 us
    dot_general x1, matrix products, one_block(): jnp.einsum('hqk,khd->qhd', exp_scores.astype(jnp.bfloat16), value_heads,...  6.67 us
    all_to_all x1, waiting for transfers between devices, per_device(): lax.all_to_all(part_means[None], 'kv', split_axis=1, concat_axis=0, tiled...  5.54 us
    all_to_all x1, starting transfers between devices, per_device(): lax.all_to_all(part_means[None], 'kv', split_axis=1, concat_axis=0, tiled...  5.1 us
    all_to_all x1, starting transfers between devices, per_device(): lax.all_to_all(part_high[None], 'kv', split_axis=1, concat_axis=0, tiled=...  4.87 us
  transfers between devices with their start and end apart: 3, of which 1 were waited for; matrix products, arithmetic and copies ran while one was open for 32% of the time, Pallas kernels for 0%

commit v1 on v0

--- a/solution.py
+++ b/solution.py
@@ -144,7 +144,12 @@
     part_means, part_high, part_mass = attend_piece(
         gathered, positions, all_keys, all_values, key_bias, key_slots, cache_len
     )
-    part_means = lax.all_to_all(part_means[None], "kv", split_axis=1, concat_axis=0, tiled=True)
+    part_means = jnp.concatenate(
+        lax.all_to_all(
+            jnp.stack(jnp.split(part_means[None], lax.axis_size("kv"), axis=1)), "kv", 0, 0
+        ),
+        axis=0,
+    )
     part_high, part_mass = (
         lax.all_to_all(part_high[None], "kv", split_axis=1, concat_axis=0, tiled=True),
         lax.all_to_all(part_mass[None], "kv", split_axis=1, concat_axis=0, tiled=True),

time: 127 us -> 109 us (0.86)
  local copies, waits for them, and re-layouts: 31.8 us -> 20.5 us
  other arithmetic: 21.8 us -> 18.7 us
  starting transfers between devices: 14 us -> 11.9 us
  waiting for transfers between devices: 5.55 us -> 3.49 us
    unnamed x4 -> x3, other arithmetic: 7.29 us -> 2.68 us
    unnamed x57 -> x34, local copies, waits for them, and re-layouts: 14.3 us -> 10.1 us
    convert_element_type x2 -> x0, local copies, waits for them, and re-layouts: 4.16 us -> none  [combine(): part_means.reshape(peer_count, row_count, head_count, -1)]
    all_to_all x1, waiting for transfers between devices: 5.54 us -> 2 us  [per_device(): lax.all_to_all(jnp.stack(jnp.split(part_means[None], lax.axis_size('kv'),...]
    another operation x8, local copies, waits for them, and re-layouts: 5.01 us -> 2.17 us
    another operation x2 -> x3, other arithmetic: 2.43 us -> 4.28 us
    all_to_all x1, starting transfers between devices: 5.1 us -> 3.61 us  [per_device(): lax.all_to_all(jnp.stack(jnp.split(part_means[None], lax.axis_size('kv'),...]
    all_to_all x1, waiting for transfers between devices: 0.01 us -> 1.48 us  [per_device(): lax.all_to_all(part_high[None], 'kv', split_axis=1, concat_axis=0, tiled=...]
  transfers between devices with their start and end apart: 3 -> 3, of which waited for: 1 -> 2; matrix products, arithmetic and copies ran while one was open for 32% -> 31% of each run, Pallas kernels for 0% -> 0%
where the time goes in v1:
time: 109 us; the launch traced here: 108 us
  blocking collectives  30.4 us (28%)
  local copies, waits for them, and re-layouts  20.5 us (19%)
  matrix products  20.3 us (19%)
  other arithmetic  18.7 us (17%)
  starting transfers between devices  11.9 us (11%)
  waiting for transfers between devices  3.49 us (3%)
  between operations  2.36 us (2%)
    all_gather x1, blocking collectives, per_device(): gathered = lax.all_gather(own_queries, 'kv', axis=0, tiled=True)  14.8 us
    unnamed x1, blocking collectives  13.5 us
    unnamed x34, local copies, waits for them, and re-layouts  10.1 us
    dot_general x1, matrix products, one_block(): jnp.einsum('hqk,khd->qhd', exp_scores.astype(jnp.bfloat16), value_heads,...  5.96 us
    all_to_all x1, starting transfers between devices, per_device(): lax.all_to_all(part_high[None], 'kv', split_axis=1, concat_axis=0, tiled=...  4.87 us
    dot_general x1, matrix products, one_block(): jnp.einsum('qhd,khd->hqk', block_q.reshape(row_count, head_count, head_wi...  3.9 us
    all_to_all x1, starting transfers between devices, per_device(): lax.all_to_all(jnp.stack(jnp.split(part_means[None], lax.axis_size('kv'),...  3.61 us
    all_to_all x1, starting transfers between devices, per_device(): lax.all_to_all(part_mass[None], 'kv', split_axis=1, concat_axis=0, tiled=...  3.43 us
  transfers between devices with their start and end apart: 3, of which 2 were waited for; matrix products, arithmetic and copies ran while one was open for 31% of the time, Pallas kernels for 0%

profile of v1, /device:TPU:0, one launch (start us, length us, event | category | flops | bytes accessed | tf_op | source)
XLA Modules:
  0.0 107.7 jit_solution(11430982527838824378)
XLA Ops:
  0.7 1.4 %fusion.9 = f32[129]{0:T(256)S(1)} fusion(bf16[1,2048]{1,0:T(2,128)(2,1)} %param.20, bf16[128,2048]{1,0:T(8,128)(2,1)} %param.19), kind=kLoop, calls=%fused_computation.16 | loop fusion | flops 1585023 | bytes 528900 | tf_op jit(solution)/shard_map/reduce_sum | solution.py:24
  2.9 1.5 %fusion.26 = f32[129,8]{0,1:T(8,128)S(1)} fusion(bf16[2048,16]{0,1:T(8,128)(2,1)} %param.25, s32[]{:T(128)S(6)} %select_n.43, f32[8]{0:T(128)S(1)} %dynamic_slice.18, f32[2048]{0:T(1024)} %param.21, f32[129]{0:T(256)S(1)} %add_rsqrt_fusion, bf16[1,2048]{1,0:T(2,128)(2,1)} %param.20, bf16[128,2048]{1,0:T(8,128)(2,1)} %param.19), kind=kOutput, calls=%fused_computation.54 | convolution fusion | flops 6085704 | bytes 578120 | tf_op jit(solution)/shard_map/dot_general | solution.py:128
  5.9 13.5 %all-reduce.1 = f32[32]{0:T(128)S(1)} all-reduce(f32[32]{0:T(128)S(1)} %dynamic-update-slice), channel_id=2, replica_groups=mesh['dp'=4,'kv'=4,'tp'=2] {'kv'}, use_global_device_ids=true, to_apply=%add.1 | all-reduce | flops 32 | bytes 256
  20.1 2.1 %convolution_convert_fusion.2 = bf16[129,512]{1,0:T(8,128)(2,1)S(1)} fusion(bf16[2048,512]{1,0:T(8,128)(2,1)} %param.23, f32[2048]{0:T(1024)S(1)} %copy-done.10, f32[129]{0:T(256)S(1)} %add_rsqrt_fusion, bf16[1,2048]{1,0:T(2,128)(2,1)S(1)} %copy-done.8, bf16[128,2048]{1,0:T(8,128)(2,1)S(1)} %copy-done.3), kind=kOutput, calls=%fused_computation.14 | convolution fusion | flops 272448000 | bytes 2766340 | tf_op jit(solution)/shard_map/dot_general | solution.py:120
  23.4 2.3 %convolution_convert_fusion.3 = bf16[129,512]{1,0:T(8,128)(2,1)S(1)} fusion(bf16[2048,512]{1,0:T(8,128)(2,1)} %param.22, f32[2048]{0:T(1024)S(1)} %copy-done.10, f32[129]{0:T(256)S(1)} %add_rsqrt_fusion, bf16[1,2048]{1,0:T(2,128)(2,1)S(1)} %copy-done.8, bf16[128,2048]{1,0:T(8,128)(2,1)} %param.19), kind=kOutput, calls=%fused_computation.15 | convolution fusion | flops 272448000 | bytes 2766340 | tf_op jit(solution)/shard_map/dot_general | solution.py:119
  26.3 14.8 %all_gather.12 = bf16[512,512]{1,0:T(8,128)(2,1)S(1)} all-gather(bf16[128,512]{1,0:T(8,128)(2,1)S(1)} %slice.52), channel_id=1, replica_groups=mesh['dp'=4,'kv'=4,'tp'=2] {'kv'}, dimensions={0}, use_global_device_ids=true | all-gather | bytes 655360 | tf_op jit(solution)/shard_map/all_gather | solution.py:142
  42.2 3.9 %fusion.2 = (f32[8,512]{1,0:T(8,128)S(1)}, f32[8,512,640]{2,1,0:T(8,128)S(1)}) fusion(f32[8,640]{1,0:T(8,128)S(1)} %maximum_negate_fusion, pred[512,640]{1,0:T(8,128)(4,1)S(1)} %concatenate.22, bf16[512,8,64]{0,2,1:T(8,128)(2,1)} %bitcast.100, bf16[640,8,64]{0,2,1:T(8,128)(2,1)} %bitcast.97), kind=kOutput, calls=%fused_computation.6 | convolution fusion | flops 346025984 | bytes 12029952 | tf_op jit(solution)/shard_map/qhd,khd->hqk/dot_general | solution.py:40
  46.1 2.9 %fusion.1 = f32[8,512]{1,0:T(8,128)S(1)} fusion(f32[8,512,640]{2,1,0:T(8,128)S(1)} %get-tuple-element.120, f32[8,512]{1,0:T(8,128)S(1)} %get-tuple-element.119, f32[8,640]{1,0:T(8,128)S(1)} %maximum_negate_fusion, pred[512,640]{1,0:T(8,128)(4,1)S(1)} %concatenate.22), kind=kLoop, calls=%fused_computation.5 | loop fusion | flops 13103104 | bytes 10866688 | tf_op jit(solution)/shard_map/reduce_sum | solution.py:56
  50.8 1.3 %reduce.20 = f32[512,8]{1,0:T(8,128)S(1)} reduce(f32[512,1,8]{2,1,0:T(1,128)S(1)} %bitcast.94, f32[]{:T(128)} %broadcast.110), dimensions={1}, to_apply=%bitcast.68.reduce_sub_computation | reduce | bytes 32772
  52.9 3.4 %all-to-all-start = ((f32[4,1,1024]{2,1,0:T(1,128)}), f32[4,1,1024]{2,1,0:T(1,128)S(1)}, u32[]{:S(2)}, u32[]{:S(2)}) async-start(f32[4,1,1024]{2,1,0:T(1,128)} %reshape.251), calls=%async_computation | async-start | bytes 32768 | tf_op jit(solution)/shard_map/all_to_all | solution.py:155
  57.2 2.3 %reduce-window.6 = f32[1,8,8,128]{3,2,1,0:T(8,128)S(1)} reduce-window(f32[1,8,8,128]{3,2,1,0:T(8,128)S(1)} %copy.76, f32[]{:T(128)} %constant.56.clone.1), window={size=1x1x1x128 pad=0_0x0_0x0_0x127_0}, to_apply=%region_10.11 | reduce-window | flops 1040384 | bytes 65540 | tf_op jit(solution)/shard_map/reduce-window
  61.6 2.3 %convolution_convert_fusion.1 = bf16[129,512]{1,0:T(8,128)(2,1)S(1)} fusion(bf16[2048,512]{1,0:T(8,128)(2,1)} %param.24, f32[2048]{0:T(1024)S(1)} %copy-done.10, f32[129]{0:T(256)S(1)} %add_rsqrt_fusion, bf16[1,2048]{1,0:T(2,128)(2,1)S(1)} %copy-done.8, bf16[128,2048]{1,0:T(8,128)(2,1)} %param.19), kind=kOutput, calls=%fused_computation.13 | convolution fusion | flops 272448000 | bytes 2766340 | tf_op jit(solution)/shard_map/dot_general | solution.py:121
  66.7 6.0 %divide_convert_fusion = bf16[512,8,64]{0,2,1:T(8,128)(2,1)S(1)} fusion(bf16[640,8,64]{0,2,1:T(8,128)(2,1)} %bitcast.98, f32[8,512,640]{2,1,0:T(8,128)} %copy-done.1, f32[8,512]{1,0:T(8,128)S(1)} %get-tuple-element.119, f32[8,640]{1,0:T(8,128)S(1)} %maximum_negate_fusion, pred[512,640]{1,0:T(8,128)(4,1)S(1)} %concatenate.22, f32[512,8]{0,1:T(8,128)S(1)} %bitcast.105), kind=kOutput, calls=%fused_computation.22 | convolution fusion | flops 349175808 | bytes 12046336 | tf_op jit(solution)/shard_map/hqk,khd->qhd/dot_general | solution.py:57
  73.7 1.5 %copy.75 = bf16[1,1024,512]{1,2,0:T(8,128)(2,1)S(1)} copy(bf16[1,1024,512]{2,1,0:T(8,128)(2,1)} %param.32) | data formatting | bytes 2097152 | tf_op args[13]
  76.9 1.3 %reduce.22 = f32[512,8]{1,0:T(8,128)S(1)} reduce(f32[512,1,8]{2,1,0:T(1,128)S(1)} %bitcast.95, f32[]{:T(128)} %broadcast.110), dimensions={1}, to_apply=%bitcast.70.reduce_sub_computation | reduce | bytes 32772
  79.0 4.9 %all-to-all-start.1 = ((f32[4,1,1024]{2,1,0:T(1,128)}), f32[4,1,1024]{2,1,0:T(1,128)S(1)}, u32[]{:S(2)}, u32[]{:S(2)}) async-start(f32[4,1,1024]{2,1,0:T(1,128)} %reshape.253), calls=%async_computation.1 | async-start | bytes 32768 | tf_op jit(solution)/shard_map/all_to_all | solution.py:154
  83.9 1.9 %pad_maximum_fusion.3 = bf16[4,1,128,512]{2,3,1,0:T(8,128)(2,1)} fusion(bf16[1,1,128,512]{2,3,1,0:T(8,128)(2,1)S(1)} %get-tuple-element.110, bf16[1,1,128,512]{2,3,1,0:T(8,128)(2,1)} %get-tuple-element.111, bf16[1,1,128,512]{2,3,1,0:T(8,128)(2,1)} %get-tuple-element.112, bf16[1,1,128,512]{2,3,1,0:T(8,128)(2,1)S(1)} %get-tuple-element.109), kind=kLoop, calls=%fused_computation.26 | loop fusion | flops 786432 | bytes 1048576 | tf_op jit(solution)/shard_map/stack | solution.py:149
  85.7 2.3 %copy.80 = bf16[1,1024,512]{1,2,0:T(8,128)(2,1)} copy(bf16[1,1024,512]{2,1,0:T(8,128)(2,1)} %param.33) | data formatting | bytes 2097152 | tf_op args[14]
  88.0 1.5 %all-to-all-done.1 = f32[4,1,1024]{2,1,0:T(1,128)S(1)} async-done(((f32[4,1,1024]{2,1,0:T(1,128)}), f32[4,1,1024]{2,1,0:T(1,128)S(1)}, u32[]{:S(2)}, u32[]{:S(2)}) %all-to-all-start.1) | async-done | bytes 16416 | tf_op jit(solution)/shard_map/all_to_all | solution.py:154
  89.5 3.6 %all-to-all-start.2 = ((bf16[4,1,128,512]{2,3,1,0:T(8,128)(2,1)}), bf16[4,1,128,512]{2,3,1,0:T(8,128)(2,1)S(1)}, u32[]{:S(2)}, u32[]{:S(2)}) async-start(bf16[4,1,128,512]{2,3,1,0:T(8,128)(2,1)} %pad_maximum_fusion.3), calls=%async_computation.2 | async-start | bytes 1048576 | tf_op jit(solution)/shard_map/all_to_all | solution.py:148
  93.9 1.6 %fusion.20 = f32[8,1,64]{2,1,0:T(1,128)S(1)} fusion(bf16[1024,8,64]{0,2,1:T(8,128)(2,1)} %bitcast.96, bf16[8,1024,1]{1,0,2:T(8,128)(2,1)S(1)} %get-tuple-element.114), kind=kOutput, calls=%fused_computation.44 | convolution fusion | flops 1048576 | bytes 1067008 | tf_op jit(solution)/shard_map/bhl,blhd->bhd/dot_general | solution.py:185
  98.9 1.5 %fusion.40 = (f32[128,8]{1,0:T(8,128)}, f32[4,128,8]{2,1,0:T(8,128)S(1)}) fusion(f32[4,128,8]{2,1,0:T(8,128)S(1)} %bitcast.93, f32[4,128,8]{2,1,0:T(8,128)S(1)} %bitcast.92, f32[128,8]{1,0:T(8,128)} %reduce_max.28), kind=kLoop, calls=%fused_computation.78 | loop fusion | flops 11264 | bytes 57344 | tf_op jit(solution)/shard_map/reduce_sum | solution.py:88
  101.4 2.0 %all-to-all-done.2 = bf16[4,1,128,512]{2,3,1,0:T(8,128)(2,1)S(1)} async-done(((bf16[4,1,128,512]{2,3,1,0:T(8,128)(2,1)}), bf16[4,1,128,512]{2,3,1,0:T(8,128)(2,1)S(1)}, u32[]{:S(2)}, u32[]{:S(2)}) %all-to-all-start.2) | async-done | bytes 524320 | tf_op jit(solution)/shard_map/all_to_all | solution.py:148
  103.7 2.2 %all_gather.15 = bf16[129,1024]{0,1:T(8,128)(2,1)S(1)} all-gather(bf16[129,512]{0,1:T(8,128)(2,1)S(1)} %pad_maximum_fusion.4), channel_id=1, replica_groups=mesh['dp'=4,'kv'=4,'tp'=2] {'tp'}, dimensions={1}, use_global_device_ids=true | all-gather | bytes 396288 | tf_op jit(solution)/shard_map/all_gather | solution.py:201
  (100 shorter events, 23.7 us)
Async XLA Ops:
  0.6 105.2 %copy-start = (bf16[1024,1024]{1,0:T(8,128)(2,1)S(1)}, bf16[1024,1024]{1,0:T(8,128)(2,1)}, u32[]{:S(2)}) copy-start(bf16[1024,1024]{1,0:T(8,128)(2,1)} %param.27) | copy-start | bytes 6291460
  0.6 3.8 %copy-start.11 = (u32[32]{0:T(128)S(1)}, u32[32]{0:T(128)}, u32[]{:S(2)}) copy-start(u32[32]{0:T(128)} %constant.74) | copy-start | bytes 388
  0.7 19.4 %copy-start.3 = (bf16[128,2048]{1,0:T(8,128)(2,1)S(1)}, bf16[128,2048]{1,0:T(8,128)(2,1)}, u32[]{:S(2)}) copy-start(bf16[128,2048]{1,0:T(8,128)(2,1)} %param.19) | copy-start | bytes 1572868
  0.7 19.4 %copy-start.8 = (bf16[1,2048]{1,0:T(2,128)(2,1)S(1)}, bf16[1,2048]{1,0:T(2,128)(2,1)}, u32[]{:S(2)}) copy-start(bf16[1,2048]{1,0:T(2,128)(2,1)} %param.20) | copy-start | bytes 12292
  0.7 19.4 %copy-start.10 = (f32[2048]{0:T(1024)S(1)}, f32[2048]{0:T(1024)}, u32[]{:S(2)}) copy-start(f32[2048]{0:T(1024)} %param.21) | copy-start | bytes 24580
  0.7 19.2 %copy-start.9 = (f32[16]{0:T(128)S(1)}, f32[16]{0:T(128)}, u32[]{:S(2)}) copy-start(f32[16]{0:T(128)} %param.31) | copy-start | bytes 196
  19.6 2.7 %copy-start.2 = (bf16[512,512]{1,0:T(8,128)(2,1)S(1)}, bf16[512,512]{1,0:T(8,128)(2,1)}, u32[]{:S(2)}) copy-start(bf16[512,512]{1,0:T(8,128)(2,1)} %param.28) | copy-start | bytes 1572868
  23.4 18.7 %copy-start.7 = (f32[8,512]{1,0:T(8,128)S(1)}, f32[8,512]{1,0:T(8,128)}, u32[]{:S(2)}) copy-start(f32[8,512]{1,0:T(8,128)} %param.30) | copy-start | bytes 49156
  25.7 0.7 copy-start.5
  46.1 4.0 %copy-start.1 = (f32[8,512,640]{2,1,0:T(8,128)}, f32[8,512,640]{2,1,0:T(8,128)S(1)}, u32[]{:S(2)}) copy-start(f32[8,512,640]{2,1,0:T(8,128)S(1)} %get-tuple-element.120) | copy-start | bytes 31457284
  46.1 11.0 %copy-start.6 = (f32[1,8,1024]{2,1,0:T(8,128)S(1)}, f32[1,8,1024]{2,1,0:T(8,128)}, u32[]{:S(2)}) copy-start(f32[1,8,1024]{2,1,0:T(8,128)} %param.34) | copy-start | bytes 98308
  52.9 26.1 %all-to-all-start = ((f32[4,1,1024]{2,1,0:T(1,128)}), f32[4,1,1024]{2,1,0:T(1,128)S(1)}, u32[]{:S(2)}, u32[]{:S(2)}) async-start(f32[4,1,1024]{2,1,0:T(1,128)} %reshape.251), calls=%async_computation | async-start | bytes 32768 | tf_op jit(solution)/shard_map/all_to_all | solution.py:155
  63.8 0.7 copy-start.4
  79.0 10.5 %all-to-all-start.1 = ((f32[4,1,1024]{2,1,0:T(1,128)}), f32[4,1,1024]{2,1,0:T(1,128)S(1)}, u32[]{:S(2)}, u32[]{:S(2)}) async-start(f32[4,1,1024]{2,1,0:T(1,128)} %reshape.253), calls=%async_computation.1 | async-start | bytes 32768 | tf_op jit(solution)/shard_map/all_to_all | solution.py:154
  89.5 13.9 %all-to-all-start.2 = ((bf16[4,1,128,512]{2,3,1,0:T(8,128)(2,1)}), bf16[4,1,128,512]{2,3,1,0:T(8,128)(2,1)S(1)}, u32[]{:S(2)}, u32[]{:S(2)}) async-start(bf16[4,1,128,512]{2,3,1,0:T(8,128)(2,1)} %pad_maximum_fusion.3), calls=%async_computation.2 | async-start | bytes 1048576 | tf_op jit(solution)/shard_map/all_to_all | solution.py:148
